TPU v7x, 32 devices: a whole 2x2x4 slice. The times are simulated.
32 devices in a mesh: sp: 8 (over z, y), tp: 4 (over x, core).
Axes of the slice: x: 2, y: 2, z: 4, core: 2. Of those that a mesh axis runs over, the one named last changes fastest.
Arguments:
- latents: bfloat16 [5120, 2048], P('sp'), may hold values from -6 to 6
- cond: float32 [2048], replicated, may hold values from -6 to 6
- ctx_cond: float32 [2048], replicated, may hold values from -6 to 6
- context: bfloat16 [768, 2048], P('sp'), may hold values from -6 to 6
- norm_gain: float32 [2048], replicated, may hold values from 0.1 to 1.9
- shift_weight: bfloat16 [2048, 2048], P('tp'), may hold values from -0.125 to 0.125
- scale_weight: bfloat16 [2048, 2048], P('tp'), may hold values from -0.125 to 0.125
- gate_weight: bfloat16 [2048, 2048], P('tp'), may hold values from -0.125 to 0.125
- q_weight: bfloat16 [2048, 1024], P(None, 'tp'), may hold values from -0.125 to 0.125
- k_weight: bfloat16 [2048, 1024], P(None, 'tp'), may hold values from -0.125 to 0.125
- v_weight: bfloat16 [2048, 1024], P(None, 'tp'), may hold values from -0.125 to 0.125
- out_weight: bfloat16 [1024, 2048], replicated, may hold values from -1.5 to 1.5
- rel_bias: float32 [8, 15, 31], P('tp'), may hold values from 1.5 to 260
Outputs:
- result: bfloat16 [5120, 2048], P(('sp', 'tp'))
All inputs are finite; a program needn't handle non-finite values.
Results may differ from a plain program's by a relative error of at most 0.0085.
Values may be sent and summed in bfloat16 or wider, within the bound.
A program may use at most 64 MiB of HBM per device.

v0:
```python
import jax
import jax.numpy as jnp
from jax import lax
from jax.sharding import PartitionSpec as P

HEAD_DIM = 128
GRID_W = 64
WIN_ROWS = 8
WIN_COLS = 16


EPS = 1e-06
NEG_BIG = -1e30


def with_halo(shard, sides, width):
    for axis, dim in sides:
        count, length = (lax.axis_size(axis), shard.shape[dim])
        up = [(i, (i + 1) % count) for i in range(count - 1)]
        down = [(j, i) for i, j in up]
        last = lax.slice_in_dim(shard, length - width, length, axis=dim)
        initial = lax.slice_in_dim(shard, 0, width, axis=dim)
        before = lax.ppermute(last, axis, up)
        after = lax.ppermute(initial, axis, down)
        shard = jnp.concatenate([before, shard, after], axis=dim)
    return shard


def modulated_norm(tok_rows, gain, shift_row, scale_row):
    rows_f = tok_rows.astype(jnp.float32)
    inverse = lax.rsqrt(jnp.mean(rows_f * rows_f, axis=-1, keepdims=True) + EPS)
    return (rows_f * inverse * gain * (1.0 + scale_row) + shift_row).astype(jnp.bfloat16)


def column_mask():
    columns = jnp.arange(GRID_W, dtype=jnp.int32)
    first_col = jnp.clip(columns - WIN_COLS // 2, 0, GRID_W - WIN_COLS)
    inside = (columns[None, :] >= first_col[:, None]) & (
        columns[None, :] < first_col[:, None] + WIN_COLS
    )
    return jnp.tile(inside, (1, WIN_ROWS))


def grid_bias(bias_table, row_diff):
    row_hot = (
        row_diff[:, :, None] == jnp.arange(2 * WIN_ROWS - 1, dtype=jnp.int32)[None, None, :]
    ).astype(jnp.float32)
    columns = jnp.arange(GRID_W, dtype=jnp.int32)
    col_diff = (
        jnp.clip(columns[None, :] - columns[:, None], -(WIN_COLS - 1), WIN_COLS - 1) + WIN_COLS - 1
    )
    col_hot = (
        col_diff[:, :, None] == jnp.arange(2 * WIN_COLS - 1, dtype=jnp.int32)[None, None, :]
    ).astype(jnp.float32)
    middle = jnp.einsum("rai,hij->hraj", row_hot, bias_table, precision=lax.Precision.HIGHEST)
    spread = jnp.einsum("hraj,qbj->hrqab", middle, col_hot, precision=lax.Precision.HIGHEST)
    return spread.reshape(bias_table.shape[0], row_diff.shape[0], GRID_W, WIN_ROWS * GRID_W)


def attend(query, key_win, val_win, ctx_keys, ctx_vals, bias, inside):
    factor = HEAD_DIM ** (-0.5)
    near_scores = (
        jnp.einsum("rqhd,rkhd->hrqk", query, key_win, preferred_element_type=jnp.float32) * factor
        + bias
    )
    near_scores = jnp.where(inside, near_scores, NEG_BIG)
    far_scores = (
        jnp.einsum("rqhd,lhd->hrql", query, ctx_keys, preferred_element_type=jnp.float32) * factor
    )
    row_peak = jnp.maximum(
        jnp.max(near_scores, axis=-1, keepdims=True), jnp.max(far_scores, axis=-1, keepdims=True)
    )
    near_exp = jnp.exp(near_scores - row_peak)
    far_exp = jnp.exp(far_scores - row_peak)
    denominator = jnp.sum(near_exp, axis=-1, keepdims=True) + jnp.sum(
        far_exp, axis=-1, keepdims=True
    )
    near_w = (near_exp / denominator).astype(jnp.bfloat16)
    far_w = (far_exp / denominator).astype(jnp.bfloat16)
    mixed = jnp.einsum(
        "hrqk,rkhd->rqhd", near_w, val_win, preferred_element_type=jnp.float32
    ) + jnp.einsum("hrql,lhd->rqhd", far_w, ctx_vals, preferred_element_type=jnp.float32)
    return mixed.astype(jnp.bfloat16)


def shards(
    latents,
    cond,
    ctx_cond,
    context,
    norm_gain,
    shift_weight,
    scale_weight,
    gate_weight,
    q_weight,
    k_weight,
    v_weight,
    out_weight,
    rel_bias,
):
    tp_rows = shift_weight.shape[0]
    conds = jnp.stack([cond, ctx_cond])
    active = jax.nn.silu(
        lax.dynamic_slice_in_dim(conds, lax.axis_index("tp") * tp_rows, tp_rows, 1)
    ).astype(jnp.bfloat16)
    shifts = jnp.dot(active, shift_weight, preferred_element_type=jnp.float32)
    scales = jnp.dot(active, scale_weight, preferred_element_type=jnp.float32)
    gates = jnp.dot(active[:1], gate_weight, preferred_element_type=jnp.float32)
    shifts, scales, gates = lax.psum((shifts, scales, gates), "tp")
    tok_dev = latents.shape[0]
    heads_here = q_weight.shape[1] // HEAD_DIM
    rows_here = tok_dev // GRID_W
    h_lat = modulated_norm(latents, norm_gain, shifts[0], scales[0])
    query = jnp.dot(h_lat, q_weight, preferred_element_type=jnp.float32).astype(jnp.bfloat16)
    keys = jnp.dot(h_lat, k_weight, preferred_element_type=jnp.float32).astype(jnp.bfloat16)
    values = jnp.dot(h_lat, v_weight, preferred_element_type=jnp.float32).astype(jnp.bfloat16)
    whole_ctx = lax.all_gather(context, "sp", axis=0, tiled=True)
    h_ctx = modulated_norm(whole_ctx, norm_gain, shifts[1], scales[1])
    ctx_keys = jnp.dot(h_ctx, k_weight, preferred_element_type=jnp.float32).astype(jnp.bfloat16)
    ctx_vals = jnp.dot(h_ctx, v_weight, preferred_element_type=jnp.float32).astype(jnp.bfloat16)
    ctx_count = ctx_keys.shape[0]
    ctx_keys = ctx_keys.reshape(ctx_count, heads_here, HEAD_DIM)
    ctx_vals = ctx_vals.reshape(ctx_count, heads_here, HEAD_DIM)
    half_rows = WIN_ROWS // 2
    stacked = jnp.stack([keys, values]).reshape(2, rows_here, GRID_W, heads_here * HEAD_DIM)
    padded = with_halo(stacked, (("sp", 1),), half_rows)
    base_row = lax.axis_index("sp") * rows_here
    total_rows = rows_here * lax.axis_size("sp")
    grid_rows = base_row + jnp.arange(rows_here, dtype=jnp.int32)
    first_row = jnp.clip(grid_rows - half_rows, 0, total_rows - WIN_ROWS)
    offsets = jnp.arange(WIN_ROWS, dtype=jnp.int32)
    local_index = (first_row - base_row + half_rows)[:, None] + offsets[None, :]
    windows = padded[:, local_index].reshape(2, rows_here, WIN_ROWS * GRID_W, heads_here, HEAD_DIM)
    row_diff = first_row[:, None] + offsets[None, :] - grid_rows[:, None] + WIN_ROWS - 1
    bias = grid_bias(rel_bias, row_diff)
    query_grid = query.reshape(rows_here, GRID_W, heads_here, HEAD_DIM)
    attn = attend(query_grid, windows[0], windows[1], ctx_keys, ctx_vals, bias, column_mask())
    attn = attn.reshape(tok_dev, heads_here * HEAD_DIM)
    own_rows = lax.all_to_all(attn, "tp", split_axis=0, concat_axis=1, tiled=True)
    row_count = own_rows.shape[0]
    residual = lax.dynamic_slice_in_dim(latents, lax.axis_index("tp") * row_count, row_count, 0)
    mixed = jnp.dot(own_rows, out_weight, preferred_element_type=jnp.float32)
    return (residual.astype(jnp.float32) + gates[0] * mixed).astype(jnp.bfloat16)


def solution(mesh):
    in_specs = (
        P("sp", None),
        P(),
        P(),
        P("sp", None),
        P(),
        P("tp", None),
        P("tp", None),
        P("tp", None),
        P(None, "tp"),
        P(None, "tp"),
        P(None, "tp"),
        P(),
        P("tp", None, None),
    )
    out_specs = P(("sp", "tp"), None)
    return jax.shard_map(shards, mesh=mesh, in_specs=in_specs, out_specs=out_specs, check_vma=False)
```

profile of v0, /device:TPU:9, one launch (start us, length us, event | category | flops | bytes accessed | tf_op | source)
XLA Modules:
  0.0 113.7 jit_solution(11099515179467072084)
XLA Ops:
  6.5 0.7 all-gather.2.cloned.1.call-update
  7.3 0.9 fusion.50
  8.2 0.4 fusion.55
  8.6 2.1 %fusion.56 = f32[2,2048]{1,0:T(2,128)S(1)} fusion(bf16[2,512]{1,0:T(2,128)(2,1)S(1)} %fusion.50, bf16[512,2048]{1,0:T(8,128)(2,1)} %param.18), kind=kOutput, calls=%fused_computation.84 | convolution fusion | flops 4194304 | bytes 2115584 | tf_op jit(solution)/shard_map/dot_general | solution.py:106
  10.7 0.4 fusion.51
  11.1 0.6 fusion.5
  11.7 11.1 %all-reduce = (f32[2,2048]{1,0:T(2,128)S(1)}, f32[2,2048]{1,0:T(2,128)S(1)}, f32[2048]{0:T(1024)S(1)}) all-reduce(f32[2,2048]{1,0:T(2,128)S(1)} %fusion.56, f32[2,2048]{1,0:T(2,128)S(1)} %fusion.55, f32[2048]{0:T(1024)S(1)} %bitcast.82), channel_id=1, replica_groups=mesh['sp'=8,'tp'=4] {'tp'}, use_global_device_ids=true, to_apply=%region_3.4 | all-reduce | flops 10240 | bytes 81920 | tf_op jit(solution)/shard_map/psum | solution.py:109
  22.9 2.9 %fusion.9 = bf16[640,2048]{1,0:T(8,128)(2,1)S(1)} fusion(bf16[640,2048]{1,0:T(8,128)(2,1)} %param.13, f32[2048]{0:T(1024)S(1)} %bitcast.84, f32[2048]{0:T(1024)S(1)} %bitcast.83, f32[2048]{0:T(1024)S(1)} %copy-done.9, f32[640]{0:T(1024)S(1)} %add_rsqrt_fusion.1), kind=kLoop, calls=%fused_computation.14 | loop fusion | flops 7864320 | bytes 5270016 | tf_op jit(solution)/shard_map/convert_element_type | solution.py:32
  25.8 0.9 convolution_convert_fusion.4
  26.7 0.6 copy-done.5
  27.3 0.5 copy-done.12
  27.8 0.8 convolution_convert_fusion.3
  28.7 3.1 %collective-permute-start = (bf16[2,4,64,256]{3,2,1,0:T(8,128)(2,1)S(1)}, bf16[2,4,64,256]{3,2,1,0:T(8,128)(2,1)S(1)}, u32[]{:S(2)}, u32[]{:S(2)}) collective-permute-start(bf16[2,4,64,256]{3,2,1,0:T(8,128)(2,1)S(1)} %get-tuple-element.10), channel_id=1, source_target_pairs={{0,4},{4,8},{8,12},{12,16},{16,20},{20,24},{24,28},{1,5},{5,9},{9,... | collective-permute-start | bytes 786440 | tf_op jit(solution)/shard_map/ppermute | solution.py:23
  31.9 3.0 %collective-permute-start.1 = (bf16[2,4,64,256]{3,2,1,0:T(8,128)(2,1)S(1)}, bf16[2,4,64,256]{3,2,1,0:T(8,128)(2,1)S(1)}, u32[]{:S(2)}, u32[]{:S(2)}) collective-permute-start(bf16[2,4,64,256]{3,2,1,0:T(8,128)(2,1)S(1)} %get-tuple-element.11), channel_id=1, source_target_pairs={{4,0},{8,4},{12,8},{16,12},{20,16},{24,20},{28,24},{5,1},{9,5},{13... | collective-permute-start | bytes 786440 | tf_op jit(solution)/shard_map/ppermute | solution.py:24
  35.0 0.1 reshape.218
  35.1 2.9 %convolution_convert_fusion.2 = bf16[640,256]{1,0:T(8,128)(2,1)S(1)} fusion(bf16[640,2048]{1,0:T(8,128)(2,1)} %copy-done.5, bf16[2048,256]{1,0:T(8,128)(2,1)} %param.21), kind=kOutput, calls=%fused_computation.40 | convolution fusion | flops 671252480 | bytes 3997696 | tf_op jit(solution)/shard_map/dot_general | solution.py:114
  38.0 0.1 reshape.211
  38.1 0.1 subtract_add_fusion
  38.2 0.1 fusion.46
  38.3 0.2 convolution_bitcast_fusion.1
  38.5 3.4 %convolution_bitcast_fusion = f32[2,10,64,8,64]{4,1,3,0,2:T(8,128)S(1)} fusion(f32[2,10,8,31,1]{3,1,2,0,4:T(8,128)S(1)} %convolution_bitcast_fusion.1, s32[64,64]{1,0:T(8,128)S(1)} %clamp_add_fusion), kind=kOutput, calls=%fused_computation.19 | convolution fusion | flops 243920896 | bytes 2657664 | tf_op jit(solution)/shard_map/hraj,qbj->hrqab/dot_general | solution.py:56
  41.9 3.9 %copy.24 = f32[2,10,64,8,64]{4,3,2,1,0:T(8,128)} copy(f32[2,10,64,8,64]{4,1,3,0,2:T(8,128)S(1)} %convolution_bitcast_fusion) | data formatting | bytes 5242880 | tf_op jit(solution)/shard_map/hraj,qbj->hrqab/transpose | solution.py:56
  45.8 5.1 %reshape.212 = f32[2,10,64,512]{3,2,1,0:T(8,128)} reshape(f32[2,10,64,8,64]{4,3,2,1,0:T(8,128)} %copy.24) | data formatting | bytes 5242880 | tf_op jit(solution)/shard_map/reshape | solution.py:57
  50.9 0.1 fusion.47
  51.0 0.2 tile.10
  51.2 0.2 pad_maximum_fusion
  51.3 5.7 %gather_fusion = bf16[80,2,64,256]{3,2,1,0:T(8,128)(2,1)} fusion(bf16[2,18,64,256]{3,2,1,0:T(8,128)(2,1)S(1)} %pad_maximum_fusion, s32[1024]{0:T(1024)S(1)} %pad_clamp_fusion), kind=kCustom, calls=%fused_computation | custom fusion | bytes 10486080 | tf_op jit(solution)/shard_map/gather | solution.py:133
  57.0 2.9 %copy.21 = bf16[80,2,64,256]{3,2,0,1:T(8,128)(2,1)S(1)} copy(bf16[80,2,64,256]{3,2,1,0:T(8,128)(2,1)} %gather_fusion) | data formatting | bytes 10485760 | tf_op jit(solution)/shard_map/gather | solution.py:133
  59.9 2.9 %fusion.52 = (bf16[1,10,8,64,256]{4,3,2,1,0:T(8,128)(2,1)}, bf16[1,10,8,64,256]{4,3,2,1,0:T(8,128)(2,1)}) fusion(bf16[2,10,8,64,256]{4,3,2,1,0:T(8,128)(2,1)S(1)} %bitcast.74), kind=kLoop, calls=%fused_computation.80 | loop fusion | bytes 10485760 | tf_op jit(solution)/shard_map/slice | solution.py:137
  62.8 4.9 %squeeze.9 = bf16[10,512,2,128]{3,2,1,0:T(2,128)(2,1)} reshape(bf16[1,10,8,64,256]{4,3,2,1,0:T(8,128)(2,1)} %get-tuple-element.8) | data formatting | bytes 5242880 | tf_op jit(solution)/shard_map/squeeze | solution.py:137
  67.7 4.9 %squeeze.8 = bf16[10,512,2,128]{3,2,1,0:T(2,128)(2,1)} reshape(bf16[1,10,8,64,256]{4,3,2,1,0:T(8,128)(2,1)} %get-tuple-element.9) | data formatting | bytes 5242880 | tf_op jit(solution)/shard_map/squeeze | solution.py:137
  72.6 5.2 %fusion.54 = (f32[2,10,64]{2,1,0:T(8,128)S(1)}, f32[2,10,64,512]{3,2,1,0:T(8,128)}) fusion(f32[2,10,64,512]{3,2,1,0:T(8,128)} %reshape.212, bf16[10,512,2,128]{3,2,1,0:T(2,128)(2,1)} %squeeze.9, bf16[10,64,2,128]{3,2,1,0:T(2,128)(2,1)S(1)} %reshape.211, pred[64,512]{1,0:T(8,128)(4,1)S(1)} %tile.10), kind=kOutput, calls=%fused_computation.82 | convolution fusion | flops 170392320 | bytes 8229888 | tf_op jit(solution)/shard_map/rqhd,rkhd->hrqk/dot_general | solution.py:63
  77.9 2.7 %fusion = f32[768]{0:T(1024)S(1)} fusion(bf16[768,2048]{1,0:T(8,128)(2,1)} %all-gather.2.cloned.1.call-done), kind=kLoop, calls=%fused_computation.5 | loop fusion | flops 4717824 | bytes 3148800 | tf_op jit(solution)/shard_map/reduce_sum | solution.py:31
  80.6 0.1 copy-done.4
  80.7 1.7 %convolution_convert_fusion.1 = bf16[768,256]{0,1:T(8,128)(2,1)S(1)} fusion(bf16[2048,256]{1,0:T(8,128)(2,1)S(1)} %copy-done.11, bf16[768,2048]{1,0:T(8,128)(2,1)S(1)} %copy-done.4, f32[2048]{0:T(1024)S(1)} %bitcast.90, f32[2048]{0:T(1024)S(1)} %bitcast.88, f32[2048]{0:T(1024)S(1)} %copy-done.9, f32[768]{0:T(1024)S(1)} %add_rsqrt_fusion), kind=kOutput, calls=%fused_computation.38 | convolution fusion | flops 814940160 | bytes 4615168 | tf_op jit(solution)/shard_map/dot_general | solution.py:119
  82.5 0.7 multiply_reduce_fusion
  83.2 0.9 fusion.10
  84.1 0.8 copy-done.3
  84.9 0.8 fusion.17
  85.8 1.1 fusion.23
  86.9 0.1 copy-done.13
  87.0 1.7 %convolution_convert_fusion = bf16[768,256]{0,1:T(8,128)(2,1)S(1)} fusion(bf16[2048,256]{1,0:T(8,128)(2,1)S(1)} %copy-done.13, bf16[768,2048]{1,0:T(8,128)(2,1)S(1)} %copy-done.4, f32[2048]{0:T(1024)S(1)} %bitcast.91, f32[2048]{0:T(1024)S(1)} %bitcast.89, f32[2048]{0:T(1024)S(1)} %copy-done.9, f32[768]{0:T(1024)S(1)} %add_rsqrt_fusion), kind=kOutput, calls=%fused_computation.37 | convolution fusion | flops 814940160 | bytes 4615168 | tf_op jit(solution)/shard_map/dot_general | solution.py:120
  88.7 1.4 %fusion.34 = bf16[10,64,2,128]{3,1,2,0:T(8,128)(2,1)S(1)} fusion(f32[10,64,2,128]{3,1,2,0:T(8,128)S(1)} %fusion.23, bf16[768,2,128,1]{0,2,1,3:T(8,128)(2,1)S(1)} %bitcast.92, f32[2,10,64,768]{3,2,1,0:T(8,128)S(1)} %get-tuple-element.19, f32[2,10,64]{2,1,0:T(8,128)S(1)} %add.232, f32[2,10,64]{2,1,0:T(8,128)S(1)} %max.29), kind=kOutput, calls=%fused_computation.39 | convolution fusion | flops 255918080 | bytes 5318656 | tf_op jit(solution)/shard_map/hrql,lhd->rqhd/dot_general | solution.py:82
  90.2 0.3 copy.31
  90.5 0.9 all_to_all.14
  91.5 5.3 %all-to-all-start = ((bf16[4,160,256]{2,1,0:T(8,128)(2,1)}), bf16[4,160,256]{2,1,0:T(8,128)(2,1)S(1)}, u32[]{:S(2)}, u32[]{:S(2)}) async-start(bf16[4,160,256]{2,1,0:T(8,128)(2,1)} %all_to_all.14), calls=%async_computation | async-start | bytes 655360 | tf_op jit(solution)/shard_map/all_to_all | solution.py:139
  96.8 5.7 %all-to-all-done = bf16[4,160,256]{2,1,0:T(8,128)(2,1)S(1)} async-done(((bf16[4,160,256]{2,1,0:T(8,128)(2,1)}), bf16[4,160,256]{2,1,0:T(8,128)(2,1)S(1)}, u32[]{:S(2)}, u32[]{:S(2)}) %all-to-all-start) | async-done | bytes 327712 | tf_op jit(solution)/shard_map/all_to_all | solution.py:139
  102.6 4.2 %fusion.16 = bf16[160,2048]{1,0:T(8,128)(2,1)} fusion(bf16[160,1024]{1,0:T(8,128)(2,1)S(1)} %bitcast.75, bf16[1024,2048]{1,0:T(8,128)(2,1)} %param.24, f32[2048]{0:T(1024)S(1)} %get-tuple-element.7, bf16[640,2048]{1,0:T(8,128)(2,1)} %param.13, s32[]{:T(128)S(6)} %select_n.20), kind=kOutput, calls=%fused_computation.29 | convolution fusion | flops 672399360 | bytes 5840900 | tf_op jit(solution)/shard_map/dot_general | solution.py:142
  (41 shorter events, 0.3 us)
Async XLA Ops:
  6.5 1.7 %copy-start = (bf16[512,2048]{1,0:T(8,128)(2,1)S(1)}, bf16[512,2048]{1,0:T(8,128)(2,1)}, u32[]{:S(2)}) copy-start(bf16[512,2048]{1,0:T(8,128)(2,1)} %param.19) | copy-start | bytes 6291460
  6.5 71.3 %all-gather.2.cloned.1.call-start = ((), (), s32[]{:S(2)}) async-start(), calls=%async_computation.1 | async-start | bytes 3538944 | tf_op jit(solution)/shard_map/all_gather | solution.py:117
  7.3 3.5 %copy-start.7 = (bf16[512,2048]{1,0:T(8,128)(2,1)S(1)}, bf16[512,2048]{1,0:T(8,128)(2,1)}, u32[]{:S(2)}) copy-start(bf16[512,2048]{1,0:T(8,128)(2,1)} %param.20) | copy-start | bytes 6291460
  8.6 2.5 %copy-start.2 = (bf16[640,2048]{1,0:T(8,128)(2,1)S(1)}, bf16[640,2048]{1,0:T(8,128)(2,1)}, u32[]{:S(2)}) copy-start(bf16[640,2048]{1,0:T(8,128)(2,1)} %param.13) | copy-start | bytes 7864324
  10.7 12.2 %copy-start.9 = (f32[2048]{0:T(1024)S(1)}, f32[2048]{0:T(1024)}, u32[]{:S(2)}) copy-start(f32[2048]{0:T(1024)} %param.17) | copy-start | bytes 24580
  22.9 2.9 %copy-start.10 = (bf16[2048,256]{1,0:T(8,128)(2,1)S(1)}, bf16[2048,256]{1,0:T(8,128)(2,1)}, u32[]{:S(2)}) copy-start(bf16[2048,256]{1,0:T(8,128)(2,1)} %param.22) | copy-start | bytes 3145732
  25.8 1.5 %copy-start.5 = (bf16[640,2048]{1,0:T(8,128)(2,1)}, bf16[640,2048]{1,0:T(8,128)(2,1)S(1)}, u32[]{:S(2)}) copy-start(bf16[640,2048]{1,0:T(8,128)(2,1)S(1)} %fusion.9) | copy-start | bytes 7864324
  25.8 2.0 %copy-start.12 = (bf16[2048,256]{1,0:T(8,128)(2,1)S(1)}, bf16[2048,256]{1,0:T(8,128)(2,1)}, u32[]{:S(2)}) copy-start(bf16[2048,256]{1,0:T(8,128)(2,1)} %param.23) | copy-start | bytes 3145732
  28.7 22.4 %collective-permute-start = (bf16[2,4,64,256]{3,2,1,0:T(8,128)(2,1)S(1)}, bf16[2,4,64,256]{3,2,1,0:T(8,128)(2,1)S(1)}, u32[]{:S(2)}, u32[]{:S(2)}) collective-permute-start(bf16[2,4,64,256]{3,2,1,0:T(8,128)(2,1)S(1)} %get-tuple-element.10), channel_id=1, source_target_pairs={{0,4},{4,8},{8,12},{12,16},{16,20},{20,24},{24,28},{1,5},{5,9},{9,... | collective-permute-start | bytes 786440 | tf_op jit(solution)/shard_map/ppermute | solution.py:23
  31.9 19.3 %collective-permute-start.1 = (bf16[2,4,64,256]{3,2,1,0:T(8,128)(2,1)S(1)}, bf16[2,4,64,256]{3,2,1,0:T(8,128)(2,1)S(1)}, u32[]{:S(2)}, u32[]{:S(2)}) collective-permute-start(bf16[2,4,64,256]{3,2,1,0:T(8,128)(2,1)S(1)} %get-tuple-element.11), channel_id=1, source_target_pairs={{4,0},{8,4},{12,8},{16,12},{20,16},{24,20},{28,24},{5,1},{9,5},{13... | collective-permute-start | bytes 786440 | tf_op jit(solution)/shard_map/ppermute | solution.py:24
  35.1 3.2 %copy-start.8 = (f32[2,15,31]{2,0,1:T(2,128)S(1)}, f32[2,15,31]{2,0,1:T(2,128)}, u32[]{:S(2)}) copy-start(f32[2,15,31]{2,0,1:T(2,128)} %param.25) | copy-start | bytes 11164
  72.6 8.0 %copy-start.11 = (bf16[2048,256]{1,0:T(8,128)(2,1)S(1)}, bf16[2048,256]{1,0:T(8,128)(2,1)}, u32[]{:S(2)}) copy-start(bf16[2048,256]{1,0:T(8,128)(2,1)} %param.22) | copy-start | bytes 3145732
  77.9 2.8 %copy-start.4 = (bf16[768,2048]{1,0:T(8,128)(2,1)S(1)}, bf16[768,2048]{1,0:T(8,128)(2,1)}, u32[]{:S(2)}) copy-start(bf16[768,2048]{1,0:T(8,128)(2,1)} %all-gather.2.cloned.1.call-done) | copy-start | bytes 9437188
  83.2 1.7 %copy-start.3 = (f32[2,10,64,512]{3,2,1,0:T(8,128)S(1)}, f32[2,10,64,512]{3,2,1,0:T(8,128)}, u32[]{:S(2)}) copy-start(f32[2,10,64,512]{3,2,1,0:T(8,128)} %get-tuple-element.17) | copy-start | bytes 7864324
  83.2 2.5 %copy-start.6 = (bf16[10,512,2,128]{3,2,1,0:T(2,128)(2,1)S(1)}, bf16[10,512,2,128]{3,2,1,0:T(2,128)(2,1)}, u32[]{:S(2)}) copy-start(bf16[10,512,2,128]{3,2,1,0:T(2,128)(2,1)} %squeeze.8) | copy-start | bytes 7864324
  85.8 1.2 %copy-start.13 = (bf16[2048,256]{1,0:T(8,128)(2,1)S(1)}, bf16[2048,256]{1,0:T(8,128)(2,1)}, u32[]{:S(2)}) copy-start(bf16[2048,256]{1,0:T(8,128)(2,1)} %param.23) | copy-start | bytes 3145732
  91.5 11.1 %all-to-all-start = ((bf16[4,160,256]{2,1,0:T(8,128)(2,1)}), bf16[4,160,256]{2,1,0:T(8,128)(2,1)S(1)}, u32[]{:S(2)}, u32[]{:S(2)}) async-start(bf16[4,160,256]{2,1,0:T(8,128)(2,1)} %all_to_all.14), calls=%async_computation | async-start | bytes 655360 | tf_op jit(solution)/shard_map/all_to_all | solution.py:139
  102.6 4.2 %copy-start.1 = (bf16[512,2048]{1,0:T(8,128)(2,1)S(1)}, bf16[512,2048]{1,0:T(8,128)(2,1)}, u32[]{:S(2)}) copy-start(bf16[512,2048]{1,0:T(8,128)(2,1)} %param.19) | copy-start | bytes 6291460
Sparse Core Ops, SparseCore 0:
  9.5 63.7 all-gather.1
where the time goes:
time: 115 us; the launch traced here: 114 us
  local copies, waits for them, and re-layouts  34 us (30%)
  matrix products  27.3 us (24%)
  between operations  13.8 us (12%)
  starting transfers between devices  11.5 us (10%)
  blocking collectives  11.1 us (10%)
  other arithmetic  9.42 us (8%)
  waiting for transfers between devices  6.46 us (6%)
    psum x1, blocking collectives, shards(): shifts, scales, gates = lax.psum((shifts, scales, gates), 'tp')  11.1 us
    gather x2, local copies, waits for them, and re-layouts, shards(): padded[:, local_index]  8.58 us
    all_to_all x1, waiting for transfers between devices, shards(): lax.all_to_all(attn, 'tp', split_axis=0, concat_axis=1, tiled=True)  5.74 us
    all_to_all x1, starting transfers between devices, shards(): lax.all_to_all(attn, 'tp', split_axis=0, concat_axis=1, tiled=True)  5.32 us
    dot_general x1, matrix products, attend(): jnp.einsum('rqhd,rkhd->hrqk', query, key_win, preferred_element_type=jnp....  5.25 us
    reshape x1, local copies, waits for them, and re-layouts, grid_bias(): spread.reshape(bias_table.shape[0], row_diff.shape[0], GRID_W, WIN_ROWS *...  5.06 us
    squeeze x1, local copies, waits for them, and re-layouts, shards(): windows[1]  4.91 us
    squeeze x1, local copies, waits for them, and re-layouts, shards(): windows[0]  4.89 us
  transfers between devices with their start and end apart: 4, of which 1 were waited for; matrix products, arithmetic and copies ran while one was open for 46% of the time, Pallas kernels for 0%

commit v1 on v0

v1 whole, which is shorter than its diff:
```python
import functools

import jax
import jax.numpy as jnp
from jax import lax
from jax.experimental import pallas as pl
from jax.experimental.pallas import tpu as pltpu
from jax.sharding import PartitionSpec as P

HEAD_DIM = 128
GRID_W = 64
WIN_ROWS = 8
WIN_COLS = 16
EPS = 1e-06
NEG_BIG = -1e30
F32 = jnp.float32
BF16 = jnp.bfloat16
UP_ROWS = WIN_ROWS // 2
DOWN_ROWS = WIN_ROWS // 2 - 1
TILE = 128
PAIR = 2 * GRID_W


def dot(a, b):
    return jnp.dot(a, b, preferred_element_type=F32)


def dot_t(a, b):
    return lax.dot_general(a, b, (((1,), (1,)), ((), ())), preferred_element_type=F32)


def kernel(
    ns, nt,
    conds, gain, table,
    lat_h, ctx_h, wsh_h, wsc_h, wg_h, wq_h, wk_h, wv_h, wo_h,
    out,
    lat, ctx, wsh, wsc, wg, wqkv, wo,
    modr, gater, mods, ctx_all, kv, q, bias, o_far, m_far, l_far, att, own,
    load_sem, mod_s, mod_r, gate_s, gate_r, ctx_s, ctx_r, halo_s, halo_r, head_s, head_r,
):
    sp, tp = lax.axis_index("sp"), lax.axis_index("tp")
    tokens, d = lat.shape
    c_here = ctx.shape[0]
    width = q.shape[1]
    heads = width // HEAD_DIM
    kt = wsh.shape[0]
    rows = tokens // GRID_W
    total_rows = rows * ns
    own_n = tokens // nt
    up_n, down_n = UP_ROWS * GRID_W, DOWN_ROWS * GRID_W
    factor = HEAD_DIM ** -0.5

    loads = [
        pltpu.make_async_copy(s, t, load_sem.at[i])
        for i, (s, t) in enumerate([
            (wsh_h, wsh), (wsc_h, wsc), (ctx_h, ctx),
            (wk_h, wqkv.at[:, pl.ds(0, width)]), (wv_h, wqkv.at[:, pl.ds(width, width)]),
            (lat_h, lat), (wq_h, wqkv.at[:, pl.ds(2 * width, width)]), (wg_h, wg), (wo_h, wo),
        ])
    ]
    for c in loads:
        c.start()

    barrier = pltpu.get_barrier_semaphore()

    def greet_tp(o, _):
        pl.semaphore_signal(barrier, inc=1, device_id={"sp": sp, "tp": (tp + o) % nt})
        return 0

    def greet_sp(o, _):
        pl.semaphore_signal(barrier, inc=1, device_id={"sp": (sp + o) % ns, "tp": tp})
        return 0

    lax.fori_loop(1, nt, greet_tp, 0)
    lax.fori_loop(1, ns, greet_sp, 0)

    start = pl.multiple_of(tp * kt, 128)
    v = conds[:, pl.ds(start, kt)]
    act = v / (1.0 + jnp.exp(-v))
    row = lax.broadcasted_iota(jnp.int32, (8, kt), 0)
    mixed_act, row0_act = act[:8], act[8:]

    def only(a, keep):
        return jnp.where(keep, a, 0.0).astype(BF16)

    loads[0].wait()
    loads[1].wait()
    half_d = d // 2
    a_sh = [only(mixed_act, (row // 2) == 2 * k) for k in range(2)]
    a_sc = [only(mixed_act, (row // 2) == 2 * k + 1) for k in range(2)]
    step = 512
    for n0 in range(0, half_d, step):
        part = jnp.zeros((8, step), F32)
        for k in range(2):
            cols = pl.ds(k * half_d + n0, step)
            part = part + dot(a_sh[k], wsh[:, cols]) + dot(a_sc[k], wsc[:, cols])
        modr[tp, :, pl.ds(n0, step)] = part
    pl.semaphore_wait(barrier, nt - 1 + ns - 1)

    def tp_copy(buf, s_sem, r_sem, o):
        return pltpu.make_async_remote_copy(
            src_ref=buf.at[tp], dst_ref=buf.at[tp],
            send_sem=s_sem.at[o], recv_sem=r_sem.at[o],
            device_id={"sp": sp, "tp": (tp + o) % nt},
        )

    def start_mod(o, _):
        tp_copy(modr, mod_s, mod_r, o).start()
        return 0

    lax.fori_loop(1, nt, start_mod, 0)

    qc = lax.broadcasted_iota(jnp.int32, (GRID_W, PAIR), 0)
    kc = lax.broadcasted_iota(jnp.int32, (GRID_W, PAIR), 1) % GRID_W
    first = jnp.clip(qc - WIN_COLS // 2, 0, GRID_W - WIN_COLS)
    inside = (kc >= first) & (kc < first + WIN_COLS)
    for h in range(heads):
        for i in range(2 * WIN_ROWS - 2):
            line = jnp.broadcast_to(table[h, pl.ds(i, 1), :], (GRID_W, PAIR))
            rolled = pltpu.roll(line, 0, 1, stride=1, stride_axis=0)
            bias[h, i] = jnp.where(inside, rolled, NEG_BIG)

    loads[7].wait()
    seg = d // 8
    gp = jnp.zeros((8, seg), F32)
    for j in range(8):
        gp = gp + dot(only(row0_act, row == j), wg[:, pl.ds(j * seg, seg)])
    gater[tp] = gp

    def start_gate(o, _):
        tp_copy(gater, gate_s, gate_r, o).start()
        return 0

    lax.fori_loop(1, nt, start_gate, 0)

    def wait_mod(o, _):
        tp_copy(modr, mod_s, mod_r, o).wait()
        return 0

    lax.fori_loop(1, nt, wait_mod, 0)
    total = modr[0]
    for i in range(1, nt):
        total = total + modr[i]
    g = gain[...]
    for k in range(2):
        cols = pl.ds(k * half_d, half_d)
        gk = g[:, k * half_d:(k + 1) * half_d]
        mods[0:1, cols] = gk * (1.0 + total[4 * k + 2:4 * k + 3])
        mods[1:2, cols] = total[4 * k:4 * k + 1]
        mods[2:3, cols] = gk * (1.0 + total[4 * k + 3:4 * k + 4])
        mods[3:4, cols] = total[4 * k + 1:4 * k + 2]

    def norm(x, r):
        xf = x.astype(F32)
        inv = lax.rsqrt(jnp.mean(xf * xf, axis=-1, keepdims=True) + EPS)
        return (xf * inv * mods[r:r + 1, :] + mods[r + 1:r + 2, :]).astype(BF16)

    loads[2].wait()
    loads[3].wait()
    loads[4].wait()
    ctx_all[sp] = dot(norm(ctx[...], 2), wqkv[:, 0:2 * width]).astype(BF16)

    def ctx_copy(o):
        return pltpu.make_async_remote_copy(
            src_ref=ctx_all.at[sp], dst_ref=ctx_all.at[sp],
            send_sem=ctx_s.at[o], recv_sem=ctx_r.at[o],
            device_id={"sp": (sp + o) % ns, "tp": tp},
        )

    def start_ctx(o, _):
        ctx_copy(o).start()
        return 0

    lax.fori_loop(1, ns, start_ctx, 0)

    up = pltpu.make_async_remote_copy(
        src_ref=kv.at[pl.ds(tokens, up_n)], dst_ref=kv.at[pl.ds(0, up_n)],
        send_sem=halo_s.at[0], recv_sem=halo_r.at[0],
        device_id={"sp": (sp + 1) % ns, "tp": tp},
    )
    down = pltpu.make_async_remote_copy(
        src_ref=kv.at[pl.ds(up_n, down_n)], dst_ref=kv.at[pl.ds(up_n + tokens, down_n)],
        send_sem=halo_s.at[1], recv_sem=halo_r.at[1],
        device_id={"sp": (sp + ns - 1) % ns, "tp": tp},
    )
    has_next, has_prev = sp < ns - 1, sp > 0

    loads[5].wait()
    loads[6].wait()
    tiles = tokens // TILE
    up_tiles = pl.cdiv(up_n, TILE)
    down_tiles = pl.cdiv(down_n, TILE)

    def project(s, _):
        t = jnp.where(s < up_tiles, tiles - 1 - s, s - up_tiles)
        base = pl.multiple_of(t * TILE, TILE)
        h = norm(lat[pl.ds(base, TILE), :], 0)
        r = dot(h, wqkv[...]).astype(BF16)
        kv[pl.ds(base + up_n, TILE), :] = r[:, :2 * width]
        q[pl.ds(base, TILE), :] = r[:, 2 * width:]

        @pl.when((s == up_tiles - 1) & has_next)
        def _():
            up.start()

        @pl.when((s == up_tiles + down_tiles - 1) & has_prev)
        def _():
            down.start()

        return 0

    lax.fori_loop(0, tiles, project, 0)

    def wait_ctx(o, _):
        ctx_copy(o).wait()
        return 0

    lax.fori_loop(1, ns, wait_ctx, 0)

    def flat(x):
        if c_here % 16:
            return x.astype(F32).reshape(ns * c_here, HEAD_DIM).astype(BF16)
        return x.reshape(ns * c_here, HEAD_DIM)

    for h in range(heads):
        lo = h * HEAD_DIM
        ck = flat(ctx_all[:, :, lo:lo + HEAD_DIM])
        cv = flat(ctx_all[:, :, width + lo:width + lo + HEAD_DIM])

        def far(t, _):
            ids = pl.ds(pl.multiple_of(t * TILE, TILE), TILE)
            s = dot_t(q[ids, lo:lo + HEAD_DIM], ck) * factor
            m = jnp.max(s, axis=-1, keepdims=True)
            e = jnp.exp(s - m)
            l_far[h, ids, :] = jnp.sum(e, axis=-1, keepdims=True)
            m_far[h, ids, :] = m
            o_far[ids, lo:lo + HEAD_DIM] = dot(e.astype(BF16), cv)
            return 0

        lax.fori_loop(0, tiles, far, 0)

    @pl.when(has_next)
    def _():
        up.wait_send()

    @pl.when(has_prev)
    def _():
        down.wait_send()
        up.wait_recv()

    @pl.when(has_next)
    def _():
        down.wait_recv()

    half_t = nt // 2
    half_rows = rows // 2
    my_half = tp // half_t
    base_row = sp * rows

    def near(i, r0):
        r = r0 + i
        grid_row = base_row + r
        s_row = jnp.clip(grid_row - WIN_ROWS // 2, 0, total_rows - WIN_ROWS)
        i0 = s_row - grid_row + WIN_ROWS - 1
        win = pl.ds(pl.multiple_of((s_row - base_row + UP_ROWS) * GRID_W, GRID_W), WIN_ROWS * GRID_W)
        ids = pl.ds(pl.multiple_of(r * GRID_W, GRID_W), GRID_W)
        for h in range(heads):
            lo = h * HEAD_DIM
            b = jnp.concatenate([bias[h, i0 + 2 * k] for k in range(WIN_ROWS // 2)], axis=1)
            s = dot_t(q[ids, lo:lo + HEAD_DIM], kv[win, lo:lo + HEAD_DIM]) * factor + b
            mf = m_far[h, ids, :]
            m = jnp.maximum(jnp.max(s, axis=-1, keepdims=True), mf)
            e = jnp.exp(s - m)
            w = jnp.exp(mf - m)
            l = jnp.sum(e, axis=-1, keepdims=True) + w * l_far[h, ids, :]
            o = dot(e.astype(BF16), kv[win, width + lo:width + lo + HEAD_DIM])
            o = (o + w * o_far[ids, lo:lo + HEAD_DIM]) / l
            att[ids, lo:lo + HEAD_DIM] = o.astype(BF16)
        return r0

    def head_copy(src, dst):
        return pltpu.make_async_remote_copy(
            src_ref=att.at[pl.ds(pl.multiple_of(dst * own_n, 16), own_n)], dst_ref=own.at[src],
            send_sem=head_s.at[dst], recv_sem=head_r.at[src],
            device_id={"sp": sp, "tp": dst},
        )

    lax.fori_loop(0, half_rows, near, (1 - my_half) * half_rows)

    def send_other(j, _):
        head_copy(tp, (1 - my_half) * half_t + j).start()
        return 0

    lax.fori_loop(0, half_t, send_other, 0)
    lax.fori_loop(0, half_rows, near, my_half * half_rows)

    def mate(o):
        return my_half * half_t + (tp + o) % half_t

    def send_same(o, _):
        head_copy(tp, mate(o)).start()
        return 0

    lax.fori_loop(1, half_t, send_same, 0)

    def wait_gate(o, _):
        tp_copy(gater, gate_s, gate_r, o).wait()
        return 0

    lax.fori_loop(1, nt, wait_gate, 0)
    gsum = gater[0]
    for i in range(1, nt):
        gsum = gsum + gater[i]
    gates = jnp.concatenate([gsum[j:j + 1] for j in range(8)], axis=1)
    loads[8].wait()
    own[tp] = att[pl.ds(pl.multiple_of(tp * own_n, 16), own_n), :]

    def settle(o, _):
        p = (tp + o) % nt
        head_copy(tp, p).wait_send()
        head_copy(p, p).wait_recv()
        return 0

    lax.fori_loop(1, nt, settle, 0)
    a = jnp.concatenate([own[i] for i in range(nt)], axis=1)
    my_rows = pl.ds(pl.multiple_of(tp * own_n, 16), own_n)
    for n0 in range(0, d, 512):
        y = dot(a, wo[:, n0:n0 + 512])
        out[:, n0:n0 + 512] = (
            lat[my_rows, n0:n0 + 512].astype(F32) + gates[:, n0:n0 + 512] * y
        ).astype(BF16)


def shards(
    ns, nt,
    latents, cond, ctx_cond, context, norm_gain, shift_weight, scale_weight, gate_weight,
    q_weight, k_weight, v_weight, out_weight, rel_bias,
):
    tokens, d = latents.shape
    c_here = context.shape[0]
    kt = shift_weight.shape[0]
    width = q_weight.shape[1]
    heads = width // HEAD_DIM
    own_n = tokens // nt
    conds = jnp.stack([cond, ctx_cond] * 4 + [cond] * 8)
    here, after = rel_bias[:, :-1], rel_bias[:, 1:]
    reach = WIN_COLS - 1
    gap = jnp.zeros(here.shape[:2] + (GRID_W - 2 * reach - 1,), F32)
    table = jnp.concatenate([here[..., reach:], gap, after, gap, here[..., :reach]], axis=-1)
    halo = (UP_ROWS + DOWN_ROWS) * GRID_W
    vmem = pl.BlockSpec(memory_space=pltpu.VMEM)
    hbm = pl.BlockSpec(memory_space=pl.ANY)
    sem = pltpu.SemaphoreType.DMA
    return pl.pallas_call(
        functools.partial(kernel, ns, nt),
        out_shape=jax.ShapeDtypeStruct((own_n, d), BF16),
        in_specs=[vmem] * 3 + [hbm] * 9,
        out_specs=vmem,
        scratch_shapes=[
            pltpu.VMEM((tokens, d), BF16),
            pltpu.VMEM((c_here, d), BF16),
            pltpu.VMEM((kt, d), BF16),
            pltpu.VMEM((kt, d), BF16),
            pltpu.VMEM((kt, d), BF16),
            pltpu.VMEM((d, 3 * width), BF16),
            pltpu.VMEM(out_weight.shape, BF16),
            pltpu.VMEM((nt, 8, d // 2), F32),
            pltpu.VMEM((nt, 8, d // 8), F32),
            pltpu.VMEM((8, d), F32),
            pltpu.VMEM((ns, c_here, 2 * width), BF16),
            pltpu.VMEM((tokens + halo, 2 * width), BF16),
            pltpu.VMEM((tokens, width), BF16),
            pltpu.VMEM((heads, 2 * WIN_ROWS - 2, GRID_W, PAIR), F32),
            pltpu.VMEM((tokens, width), F32),
            pltpu.VMEM((heads, tokens, 1), F32),
            pltpu.VMEM((heads, tokens, 1), F32),
            pltpu.VMEM((tokens, width), BF16),
            pltpu.VMEM((nt, own_n, width), BF16),
            sem((9,)),
            sem((nt,)), sem((nt,)), sem((nt,)), sem((nt,)),
            sem((ns,)), sem((ns,)),
            sem((2,)), sem((2,)),
            sem((nt,)), sem((nt,)),
        ],
        compiler_params=pltpu.CompilerParams(
            collective_id=0, has_side_effects=True, vmem_limit_bytes=62 * 1024 * 1024
        ),
    )(
        conds, norm_gain[None], table, latents, context, shift_weight, scale_weight, gate_weight,
        q_weight, k_weight, v_weight, out_weight,
    )


def solution(mesh):
    in_specs = (
        P("sp", None),
        P(),
        P(),
        P("sp", None),
        P(),
        P("tp", None),
        P("tp", None),
        P("tp", None),
        P(None, "tp"),
        P(None, "tp"),
        P(None, "tp"),
        P(),
        P("tp", None, None),
    )
    body = functools.partial(shards, mesh.shape["sp"], mesh.shape["tp"])
    return jax.shard_map(
        body, mesh=mesh, in_specs=in_specs, out_specs=P(("sp", "tp"), None), check_vma=False
    )
```

time: 115 us -> 54.3 us (0.47)
  Pallas kernels: 0 us -> 45.5 us
  matrix products: 27.3 us -> 0 us
  local copies, waits for them, and re-layouts: 34 us -> 8.21 us
  between operations: 13.8 us -> 0.02 us
  starting transfers between devices: 11.5 us -> 0 us
  blocking collectives: 11.1 us -> 0 us
  other arithmetic: 9.42 us -> 0 us
  waiting for transfers between devices: 6.46 us -> 0 us
    pallas_call x0 -> x1, Pallas kernels: none -> 45.5 us  [shards(): pl.pallas_call(functools.partial(kernel, ns, nt), out_shape=jax.ShapeDtyp...]
    dot_general x15 -> x0, matrix products: 27.3 us -> none  [the longest x1 5.25 us: attend(): jnp.einsum('rqhd,rkhd->hrqk', query, key_win, preferred_element_type=jnp....]
    psum x1 -> x0, blocking collectives: 11.1 us -> none  [shards(): shifts, scales, gates = lax.psum((shifts, scales, gates), 'tp')]
    squeeze x2 -> x0, local copies, waits for them, and re-layouts: 9.8 us -> none  [the longest x1 4.91 us: shards(): windows[1]]
    gather x2 -> x0, local copies, waits for them, and re-layouts: 8.58 us -> none  [shards(): padded[:, local_index]]
    ppermute x2 -> x0, starting transfers between devices: 6.18 us -> none  [the longest x1 3.15 us: with_halo(): before = lax.ppermute(last, axis, up)]
    all_to_all x1 -> x0, waiting for transfers between devices: 5.74 us -> none  [shards(): lax.all_to_all(attn, 'tp', split_axis=0, concat_axis=1, tiled=True)]
    all_to_all x1 -> x0, starting transfers between devices: 5.32 us -> none  [shards(): lax.all_to_all(attn, 'tp', split_axis=0, concat_axis=1, tiled=True)]
  transfers between devices with their start and end apart: 4 -> 0, of which waited for: 1 -> 0; matrix products, arithmetic and copies ran while one was open for 46% -> 0% of each run, Pallas kernels for 0% -> 0%
where the time goes in v1:
time: 54.3 us; the launch traced here: 53.7 us
  Pallas kernels  45.5 us (84%)
  local copies, waits for them, and re-layouts  8.21 us (15%)
    pallas_call x1, Pallas kernels, shards(): pl.pallas_call(functools.partial(kernel, ns, nt), out_shape=jax.ShapeDtyp...  45.5 us
    another operation x1, local copies, waits for them, and re-layouts, shards(): conds = jnp.stack([cond, ctx_cond] * 4 + [cond] * 8)  3.31 us
    unnamed x4, local copies, waits for them, and re-layouts  2 us

profile of v1, /device:TPU:9, one launch (start us, length us, event | category | flops | bytes accessed | tf_op | source)
XLA Modules:
  0.0 53.7 jit_solution(925686223816763158)
XLA Ops:
  0.0 0.7 %slice.13 = f32[2,14,31]{2,0,1:T(2,128)S(1)} slice(f32[2,15,31]{2,0,1:T(2,128)} %param.25), slice={[0:2], [1:15], [0:31]} | slice | bytes 6944 | tf_op jit(solution)/shard_map/slice | solution.py:346
  0.7 0.8 %slice.12 = f32[2,14,16]{2,0,1:T(2,128)S(1)} slice(f32[2,15,31]{2,0,1:T(2,128)} %param.25), slice={[0:2], [0:14], [15:31]} | slice | bytes 3584 | tf_op jit(solution)/shard_map/slice | solution.py:349
  1.5 0.7 %slice.14 = f32[2,14,15]{2,0,1:T(2,128)S(1)} slice(f32[2,15,31]{2,0,1:T(2,128)} %param.25), slice={[0:2], [0:14], [0:15]} | slice | bytes 3360 | tf_op jit(solution)/shard_map/slice | solution.py:349
  2.2 0.7 %concatenate.3.table = f32[2,14,128]{2,1,0:T(8,128)} concatenate(f32[2,14,16]{2,1,0:T(8,128)S(1)} %copy.17, f32[2,14,33]{2,1,0:T(8,128)S(1)} %broadcast_in_dim.7, f32[2,14,31]{2,1,0:T(8,128)S(1)} %copy.18, f32[2,14,33]{2,1,0:T(8,128)S(1)} %broadcast_in_dim.7, f32[2,14,15]{2,1,0:T(8,128)S(1)} %copy.19), dimensions={2} | concatenate | bytes 28672 | tf_op jit(solution)/shard_map/concatenate | solution.py:349
  2.9 3.3 %stack.8.conds = f32[16,2048]{1,0:T(8,128)} concatenate(f32[1,2048]{1,0:T(1,128)} %bitcast.3, f32[1,2048]{1,0:T(1,128)} %bitcast.15, f32[1,2048]{1,0:T(1,128)} %bitcast.4, f32[1,2048]{1,0:T(1,128)} %bitcast.16, f32[1,2048]{1,0:T(1,128)} %bitcast.5, f32[1,2048]{1,0:T(1,128)} %bitcast.17, f32[1,2048]{1,0:T(1,128)} %bitcast.6, f32[1,2048]{1,0:T(1,128)} %bitcast.18, ...), dimensions={0} | concatenate | bytes 262144 | tf_op jit(solution)/shard_map/stack | solution.py:345
  6.2 45.5 %shard_map.127 = bf16[160,2048]{1,0:T(8,128)(2,1)} custom-call(f32[16,2048]{1,0:T(8,128)} %stack.8.conds, f32[1,2048]{1,0:T(1,128)} %bitcast.19, f32[2,14,128]{2,1,0:T(8,128)} %concatenate.3.table, bf16[640,2048]{1,0:T(8,128)(2,1)} %lat_h.1, bf16[96,2048]{1,0:T(8,128)(2,1)} %ctx_h.1, bf16[512,2048]{1,0:T(8,128)(2,1)} %wsh_h.1, bf16[512,2048]{1,0:T(8,128)(2,1)} %wsc_h.1, ...), custom_call_target="tpu_custom_call" | custom-call | tf_op jit(solution)/shard_map/pallas_call | solution.py:354
  51.8 2.0 %copy.21 = bf16[160,2048]{1,0:T(8,128)(2,1)} copy(bf16[160,2048]{1,0:T(8,128)(2,1)} %shard_map.127) | data formatting | bytes 1310720
  (4 shorter events, 0.0 us)

commit v2 on v1

--- a/solution.py
+++ b/solution.py
@@ -19,6 +19,7 @@
 DOWN_ROWS = WIN_ROWS // 2 - 1
 TILE = 128
 PAIR = 2 * GRID_W
+VMEM_BYTES = 67043328
 
 
 def dot(a, b):
@@ -30,12 +31,12 @@
 
 
 def kernel(
-    ns, nt,
-    conds, gain, table,
+    ns, nt, ny,
+    cond, ctx_cond, gain, table,
     lat_h, ctx_h, wsh_h, wsc_h, wg_h, wq_h, wk_h, wv_h, wo_h,
     out,
     lat, ctx, wsh, wsc, wg, wqkv, wo,
-    modr, gater, mods, ctx_all, kv, q, bias, o_far, m_far, l_far, att, own,
+    modr, gater, mods, ctx_all, kv, q, bias, o_near, m_near, l_near, att, own, lines,
     load_sem, mod_s, mod_r, gate_s, gate_r, ctx_s, ctx_r, halo_s, halo_r, head_s, head_r,
 ):
     sp, tp = lax.axis_index("sp"), lax.axis_index("tp")
@@ -48,7 +49,8 @@
     total_rows = rows * ns
     own_n = tokens // nt
     up_n, down_n = UP_ROWS * GRID_W, DOWN_ROWS * GRID_W
-    factor = HEAD_DIM ** -0.5
+    to_log2 = 1.4426950408889634
+    q_scale = HEAD_DIM ** -0.5 * to_log2
 
     loads = [
         pltpu.make_async_copy(s, t, load_sem.at[i])
@@ -75,10 +77,14 @@
     lax.fori_loop(1, ns, greet_sp, 0)
 
     start = pl.multiple_of(tp * kt, 128)
-    v = conds[:, pl.ds(start, kt)]
-    act = v / (1.0 + jnp.exp(-v))
     row = lax.broadcasted_iota(jnp.int32, (8, kt), 0)
-    mixed_act, row0_act = act[:8], act[8:]
+
+    def silu(ref):
+        v = ref[:, pl.ds(start, kt)]
+        return jnp.broadcast_to(v / (1.0 + jnp.exp(-v)), (8, kt))
+
+    row0_act = silu(cond)
+    mixed_act = jnp.where(row % 2 == 0, row0_act, silu(ctx_cond))
 
     def only(a, keep):
         return jnp.where(keep, a, 0.0).astype(BF16)
@@ -114,11 +120,16 @@
     kc = lax.broadcasted_iota(jnp.int32, (GRID_W, PAIR), 1) % GRID_W
     first = jnp.clip(qc - WIN_COLS // 2, 0, GRID_W - WIN_COLS)
     inside = (kc >= first) & (kc < first + WIN_COLS)
+    lines[...] = jnp.zeros_like(lines)
+    lines[:, :, 0:2 * WIN_COLS - 1] = table[...]
     for h in range(heads):
         for i in range(2 * WIN_ROWS - 2):
-            line = jnp.broadcast_to(table[h, pl.ds(i, 1), :], (GRID_W, PAIR))
-            rolled = pltpu.roll(line, 0, 1, stride=1, stride_axis=0)
-            bias[h, i] = jnp.where(inside, rolled, NEG_BIG)
+            near_line = jnp.broadcast_to(lines[i, h:h + 1, :], (GRID_W, PAIR))
+            next_line = jnp.broadcast_to(lines[i + 1, h:h + 1, :], (GRID_W, PAIR))
+            reach = WIN_COLS - 1
+            rolled = pltpu.roll(near_line, PAIR - reach, 1, stride=1, stride_axis=0)
+            rolled = rolled + pltpu.roll(next_line, GRID_W - reach, 1, stride=1, stride_axis=0)
+            bias[h, i] = jnp.where(inside, rolled * to_log2, NEG_BIG)
 
     loads[7].wait()
     seg = d // 8
@@ -160,18 +171,58 @@
     loads[4].wait()
     ctx_all[sp] = dot(norm(ctx[...], 2), wqkv[:, 0:2 * width]).astype(BF16)
 
-    def ctx_copy(o):
+    nz = ns // ny
+    zi, yi = sp // ny, sp % ny
+
+    def ctx_copy(block, dest, lane):
         return pltpu.make_async_remote_copy(
-            src_ref=ctx_all.at[sp], dst_ref=ctx_all.at[sp],
-            send_sem=ctx_s.at[o], recv_sem=ctx_r.at[o],
-            device_id={"sp": (sp + o) % ns, "tp": tp},
+            src_ref=ctx_all.at[block], dst_ref=ctx_all.at[block],
+            send_sem=ctx_s.at[lane, block // ny], recv_sem=ctx_r.at[block],
+            device_id={"sp": dest, "tp": tp},
         )
 
-    def start_ctx(o, _):
-        ctx_copy(o).start()
-        return 0
-
-    lax.fori_loop(1, ns, start_ctx, 0)
+    def across(zb, act):
+        def one(o, _):
+            act(ctx_copy(zb * ny + yi, zi * ny + (yi + o) % ny, 1 + o))
+            return 0
+
+        lax.fori_loop(1, ny, one, 0)
+
+    def upward(zb, act):
+        @pl.when(zi < nz - 1)
+        def _():
+            act(ctx_copy(zb * ny + yi, sp + ny, 0))
+
+    def downward(zb, act):
+        @pl.when(zi > 0)
+        def _():
+            act(ctx_copy(zb * ny + yi, sp - ny, 1))
+
+    def go(c):
+        c.start()
+
+    def sent(c):
+        c.wait_send()
+
+    def arrived(block):
+        ctx_copy(block, sp, 0).wait_recv()
+
+    def relay(k):
+        @pl.when(zi - k >= 0)
+        def _():
+            arrived((zi - k) * ny + yi)
+            upward(zi - k, go)
+            across(zi - k, go)
+
+        @pl.when(zi + k < nz)
+        def _():
+            arrived((zi + k) * ny + yi)
+            downward(zi + k, go)
+            across(zi + k, go)
+
+    upward(zi, go)
+    downward(zi, go)
+    across(zi, go)
 
     up = pltpu.make_async_remote_copy(
         src_ref=kv.at[pl.ds(tokens, up_n)], dst_ref=kv.at[pl.ds(0, up_n)],
@@ -195,9 +246,9 @@
         t = jnp.where(s < up_tiles, tiles - 1 - s, s - up_tiles)
         base = pl.multiple_of(t * TILE, TILE)
         h = norm(lat[pl.ds(base, TILE), :], 0)
-        r = dot(h, wqkv[...]).astype(BF16)
-        kv[pl.ds(base + up_n, TILE), :] = r[:, :2 * width]
-        q[pl.ds(base, TILE), :] = r[:, 2 * width:]
+        r = dot(h, wqkv[...])
+        kv[pl.ds(base + up_n, TILE), :] = r[:, :2 * width].astype(BF16)
+        q[pl.ds(base, TILE), :] = (r[:, 2 * width:] * q_scale).astype(BF16)
 
         @pl.when((s == up_tiles - 1) & has_next)
         def _():
@@ -211,49 +262,7 @@
 
     lax.fori_loop(0, tiles, project, 0)
 
-    def wait_ctx(o, _):
-        ctx_copy(o).wait()
-        return 0
-
-    lax.fori_loop(1, ns, wait_ctx, 0)
-
-    def flat(x):
-        if c_here % 16:
-            return x.astype(F32).reshape(ns * c_here, HEAD_DIM).astype(BF16)
-        return x.reshape(ns * c_here, HEAD_DIM)
-
-    for h in range(heads):
-        lo = h * HEAD_DIM
-        ck = flat(ctx_all[:, :, lo:lo + HEAD_DIM])
-        cv = flat(ctx_all[:, :, width + lo:width + lo + HEAD_DIM])
-
-        def far(t, _):
-            ids = pl.ds(pl.multiple_of(t * TILE, TILE), TILE)
-            s = dot_t(q[ids, lo:lo + HEAD_DIM], ck) * factor
-            m = jnp.max(s, axis=-1, keepdims=True)
-            e = jnp.exp(s - m)
-            l_far[h, ids, :] = jnp.sum(e, axis=-1, keepdims=True)
-            m_far[h, ids, :] = m
-            o_far[ids, lo:lo + HEAD_DIM] = dot(e.astype(BF16), cv)
-            return 0
-
-        lax.fori_loop(0, tiles, far, 0)
-
-    @pl.when(has_next)
-    def _():
-        up.wait_send()
-
-    @pl.when(has_prev)
-    def _():
-        down.wait_send()
-        up.wait_recv()
-
-    @pl.when(has_next)
-    def _():
-        down.wait_recv()
-
     half_t = nt // 2
-    half_rows = rows // 2
     my_half = tp // half_t
     base_row = sp * rows
 
@@ -267,16 +276,84 @@
         for h in range(heads):
             lo = h * HEAD_DIM
             b = jnp.concatenate([bias[h, i0 + 2 * k] for k in range(WIN_ROWS // 2)], axis=1)
-            s = dot_t(q[ids, lo:lo + HEAD_DIM], kv[win, lo:lo + HEAD_DIM]) * factor + b
-            mf = m_far[h, ids, :]
-            m = jnp.maximum(jnp.max(s, axis=-1, keepdims=True), mf)
-            e = jnp.exp(s - m)
-            w = jnp.exp(mf - m)
-            l = jnp.sum(e, axis=-1, keepdims=True) + w * l_far[h, ids, :]
-            o = dot(e.astype(BF16), kv[win, width + lo:width + lo + HEAD_DIM])
-            o = (o + w * o_far[ids, lo:lo + HEAD_DIM]) / l
-            att[ids, lo:lo + HEAD_DIM] = o.astype(BF16)
+            s = dot_t(q[ids, lo:lo + HEAD_DIM], kv[win, lo:lo + HEAD_DIM]) + b
+            m = jnp.max(s, axis=-1, keepdims=True)
+            e = jnp.exp2(s - m)
+            l_near[h, ids, :] = jnp.sum(e, axis=-1, keepdims=True)
+            m_near[h, ids, :] = m
+            o_near[ids, lo:lo + HEAD_DIM] = dot(
+                e.astype(BF16), kv[win, width + lo:width + lo + HEAD_DIM]
+            )
         return r0
+
+    relay(1)
+    mid = rows - UP_ROWS - DOWN_ROWS
+    lax.fori_loop(0, mid, near, UP_ROWS, unroll=True)
+    if nz > 2:
+        relay(2)
+
+    @pl.when(has_next)
+    def _():
+        down.wait_recv()
+        up.wait_send()
+
+    @pl.when(has_prev)
+    def _():
+        up.wait_recv()
+        down.wait_send()
+
+    lax.fori_loop(0, DOWN_ROWS, near, rows - DOWN_ROWS, unroll=True)
+    if nz > 3:
+        relay(3)
+    lax.fori_loop(0, UP_ROWS, near, 0, unroll=True)
+
+    def late_relay(k, _):
+        relay(k)
+        return 0
+
+    lax.fori_loop(4, nz, late_relay, 0)
+
+    def settle_row(zb, _):
+        def other(o, _):
+            arrived(zb * ny + (yi + o) % ny)
+            return 0
+
+        lax.fori_loop(1, ny, other, 0)
+        across(zb, sent)
+
+        @pl.when(zb <= zi)
+        def _():
+            upward(zb, sent)
+
+        @pl.when(zb >= zi)
+        def _():
+            downward(zb, sent)
+
+        return 0
+
+    lax.fori_loop(0, nz, settle_row, 0)
+
+    def flat(x):
+        if c_here % 16:
+            return x.astype(F32).reshape(ns * c_here, HEAD_DIM).astype(BF16)
+        return x.reshape(ns * c_here, HEAD_DIM)
+
+    far_tile = tokens // 4
+
+    def far(t):
+        ids = pl.ds(pl.multiple_of(t * far_tile, 16), far_tile)
+        for h in range(heads):
+            lo = h * HEAD_DIM
+            ck = flat(ctx_all[:, :, lo:lo + HEAD_DIM])
+            cv = flat(ctx_all[:, :, width + lo:width + lo + HEAD_DIM])
+            s = dot_t(q[ids, lo:lo + HEAD_DIM], ck)
+            mn = m_near[h, ids, :]
+            m = jnp.maximum(jnp.max(s, axis=-1, keepdims=True), mn)
+            e = jnp.exp2(s - m)
+            w = jnp.exp2(mn - m)
+            l = jnp.sum(e, axis=-1, keepdims=True) + w * l_near[h, ids, :]
+            o = dot(e.astype(BF16), cv) + w * o_near[ids, lo:lo + HEAD_DIM]
+            att[ids, lo:lo + HEAD_DIM] = (o / l).astype(BF16)
 
     def head_copy(src, dst):
         return pltpu.make_async_remote_copy(
@@ -285,14 +362,16 @@
             device_id={"sp": sp, "tp": dst},
         )
 
-    lax.fori_loop(0, half_rows, near, (1 - my_half) * half_rows)
+    far((1 - my_half) * 2)
+    far((1 - my_half) * 2 + 1)
 
     def send_other(j, _):
         head_copy(tp, (1 - my_half) * half_t + j).start()
         return 0
 
     lax.fori_loop(0, half_t, send_other, 0)
-    lax.fori_loop(0, half_rows, near, my_half * half_rows)
+    far(my_half * 2)
+    far(my_half * 2 + 1)
 
     def mate(o):
         return my_half * half_t + (tp + o) % half_t
@@ -342,19 +421,18 @@
     width = q_weight.shape[1]
     heads = width // HEAD_DIM
     own_n = tokens // nt
-    conds = jnp.stack([cond, ctx_cond] * 4 + [cond] * 8)
-    here, after = rel_bias[:, :-1], rel_bias[:, 1:]
-    reach = WIN_COLS - 1
-    gap = jnp.zeros(here.shape[:2] + (GRID_W - 2 * reach - 1,), F32)
-    table = jnp.concatenate([here[..., reach:], gap, after, gap, here[..., :reach]], axis=-1)
+    table = jnp.transpose(rel_bias, (1, 0, 2))
+    ny = 1
+    while ns % (2 * ny) == 0 and 4 * ny * ny <= ns:
+        ny *= 2
     halo = (UP_ROWS + DOWN_ROWS) * GRID_W
     vmem = pl.BlockSpec(memory_space=pltpu.VMEM)
-    hbm = pl.BlockSpec(memory_space=pl.ANY)
+    hbm = pl.BlockSpec(memory_space=pltpu.HBM)
     sem = pltpu.SemaphoreType.DMA
     return pl.pallas_call(
-        functools.partial(kernel, ns, nt),
+        functools.partial(kernel, ns, nt, ny),
         out_shape=jax.ShapeDtypeStruct((own_n, d), BF16),
-        in_specs=[vmem] * 3 + [hbm] * 9,
+        in_specs=[vmem] * 4 + [hbm] * 9,
         out_specs=vmem,
         scratch_shapes=[
             pltpu.VMEM((tokens, d), BF16),
@@ -376,17 +454,18 @@
             pltpu.VMEM((heads, tokens, 1), F32),
             pltpu.VMEM((tokens, width), BF16),
             pltpu.VMEM((nt, own_n, width), BF16),
+            pltpu.VMEM((2 * WIN_ROWS - 1, heads, PAIR), F32),
             sem((9,)),
             sem((nt,)), sem((nt,)), sem((nt,)), sem((nt,)),
-            sem((ns,)), sem((ns,)),
+            sem((ny + 1, ns // ny)), sem((ns,)),
             sem((2,)), sem((2,)),
             sem((nt,)), sem((nt,)),
         ],
         compiler_params=pltpu.CompilerParams(
-            collective_id=0, has_side_effects=True, vmem_limit_bytes=62 * 1024 * 1024
+            collective_id=0, has_side_effects=True, vmem_limit_bytes=VMEM_BYTES - own_n * d * 2 - 300 * 1024
         ),
     )(
-        conds, norm_gain[None], table, latents, context, shift_weight, scale_weight, gate_weight,
+        cond[None], ctx_cond[None], norm_gain[None], table, latents, context, shift_weight, scale_weight, gate_weight,
         q_weight, k_weight, v_weight, out_weight,
     )
 

time: 54.3 us -> 40.3 us (0.74)
  Pallas kernels: 45.5 us -> 37.8 us
  local copies, waits for them, and re-layouts: 8.21 us -> 1.98 us
    pallas_call x1, Pallas kernels: 45.5 us -> 37.8 us  [shards(): pl.pallas_call(functools.partial(kernel, ns, nt, ny), out_shape=jax.Shape...]
    another operation x1 -> x0, local copies, waits for them, and re-layouts: 3.31 us -> none  [shards(): conds = jnp.stack([cond, ctx_cond] * 4 + [cond] * 8)]
    slice x3 -> x0, local copies, waits for them, and re-layouts: 2.22 us -> none  [the longest x1 0.79 us: shards(): here[..., reach:]]
    concatenate x1 -> x0, local copies, waits for them, and re-layouts: 0.68 us -> none  [shards(): jnp.concatenate([here[..., reach:], gap, after, gap, here[..., :reach]],...]
    unnamed x4 -> x1, local copies, waits for them, and re-layouts: 2 us -> 1.98 us
where the time goes in v2:
time: 40.3 us; the launch traced here: 39.8 us
  Pallas kernels  37.8 us (94%)
  local copies, waits for them, and re-layouts  1.98 us (5%)
    pallas_call x1, Pallas kernels, shards(): pl.pallas_call(functools.partial(kernel, ns, nt, ny), out_shape=jax.Shape...  37.8 us
    unnamed x1, local copies, waits for them, and re-layouts  1.98 us

profile of v2, /device:TPU:9, one launch (start us, length us, event | category | flops | bytes accessed | tf_op | source)
XLA Modules:
  0.0 39.8 jit_solution(1951859816751423019)
XLA Ops:
  0.0 37.8 %shard_map.127 = bf16[160,2048]{1,0:T(8,128)(2,1)} custom-call(f32[1,2048]{1,0:T(1,128)} %bitcast.5, f32[1,2048]{1,0:T(1,128)} %bitcast.6, f32[1,2048]{1,0:T(1,128)} %bitcast.7, f32[15,2,31]{2,1,0:T(2,128)} %bitcast.4, bf16[640,2048]{1,0:T(8,128)(2,1)} %lat_h.1, bf16[96,2048]{1,0:T(8,128)(2,1)} %ctx_h.1, bf16[512,2048]{1,0:T(8,128)(2,1)} %wsh_h.1, ...), custom_call_target="tpu_custom_call" | custom-call | tf_op jit(solution)/shard_map/pallas_call | solution.py:432
  37.8 2.0 %copy.15 = bf16[160,2048]{1,0:T(8,128)(2,1)} copy(bf16[160,2048]{1,0:T(8,128)(2,1)} %shard_map.127) | data formatting | bytes 1310720

commit v3 on v2

--- a/solution.py
+++ b/solution.py
@@ -32,11 +32,12 @@
 
 def kernel(
     ns, nt, ny,
-    cond, ctx_cond, gain, table,
+    cond_h, ctx_cond_h, gain_h, table_h,
     lat_h, ctx_h, wsh_h, wsc_h, wg_h, wq_h, wk_h, wv_h, wo_h,
     out,
     lat, ctx, wsh, wsc, wg, wqkv, wo,
     modr, gater, mods, ctx_all, kv, q, bias, o_near, m_near, l_near, att, own, lines,
+    cond, ctx_cond, gain, table,
     load_sem, mod_s, mod_r, gate_s, gate_r, ctx_s, ctx_r, halo_s, halo_r, head_s, head_r,
 ):
     sp, tp = lax.axis_index("sp"), lax.axis_index("tp")
@@ -58,9 +59,10 @@
             (wsh_h, wsh), (wsc_h, wsc), (ctx_h, ctx),
             (wk_h, wqkv.at[:, pl.ds(0, width)]), (wv_h, wqkv.at[:, pl.ds(width, width)]),
             (lat_h, lat), (wq_h, wqkv.at[:, pl.ds(2 * width, width)]), (wg_h, wg), (wo_h, wo),
+            (cond_h, cond), (ctx_cond_h, ctx_cond), (gain_h, gain), (table_h, table),
         ])
     ]
-    for c in loads:
+    for c in loads[9:] + loads[:9]:
         c.start()
 
     barrier = pltpu.get_barrier_semaphore()
@@ -75,6 +77,9 @@
 
     lax.fori_loop(1, nt, greet_tp, 0)
     lax.fori_loop(1, ns, greet_sp, 0)
+
+    for c in loads[9:]:
+        c.wait()
 
     start = pl.multiple_of(tp * kt, 128)
     row = lax.broadcasted_iota(jnp.int32, (8, kt), 0)
@@ -131,19 +136,6 @@
             rolled = rolled + pltpu.roll(next_line, GRID_W - reach, 1, stride=1, stride_axis=0)
             bias[h, i] = jnp.where(inside, rolled * to_log2, NEG_BIG)
 
-    loads[7].wait()
-    seg = d // 8
-    gp = jnp.zeros((8, seg), F32)
-    for j in range(8):
-        gp = gp + dot(only(row0_act, row == j), wg[:, pl.ds(j * seg, seg)])
-    gater[tp] = gp
-
-    def start_gate(o, _):
-        tp_copy(gater, gate_s, gate_r, o).start()
-        return 0
-
-    lax.fori_loop(1, nt, start_gate, 0)
-
     def wait_mod(o, _):
         tp_copy(modr, mod_s, mod_r, o).wait()
         return 0
@@ -169,14 +161,15 @@
     loads[2].wait()
     loads[3].wait()
     loads[4].wait()
-    ctx_all[sp] = dot(norm(ctx[...], 2), wqkv[:, 0:2 * width]).astype(BF16)
+    ctx_all[sp % ny, sp // ny] = dot(norm(ctx[...], 2), wqkv[:, 0:2 * width]).astype(BF16)
 
     nz = ns // ny
     zi, yi = sp // ny, sp % ny
 
     def ctx_copy(block, dest, lane):
         return pltpu.make_async_remote_copy(
-            src_ref=ctx_all.at[block], dst_ref=ctx_all.at[block],
+            src_ref=ctx_all.at[block % ny, block // ny],
+            dst_ref=ctx_all.at[block % ny, block // ny],
             send_sem=ctx_s.at[lane, block // ny], recv_sem=ctx_r.at[block],
             device_id={"sp": dest, "tp": tp},
         )
@@ -261,6 +254,19 @@
         return 0
 
     lax.fori_loop(0, tiles, project, 0)
+
+    loads[7].wait()
+    seg = d // 8
+    gp = jnp.zeros((8, seg), F32)
+    for j in range(8):
+        gp = gp + dot(only(row0_act, row == j), wg[:, pl.ds(j * seg, seg)])
+    gater[tp] = gp
+
+    def start_gate(o, _):
+        tp_copy(gater, gate_s, gate_r, o).start()
+        return 0
+
+    lax.fori_loop(1, nt, start_gate, 0)
 
     half_t = nt // 2
     my_half = tp // half_t
@@ -313,47 +319,63 @@
 
     lax.fori_loop(4, nz, late_relay, 0)
 
-    def settle_row(zb, _):
-        def other(o, _):
-            arrived(zb * ny + (yi + o) % ny)
-            return 0
-
-        lax.fori_loop(1, ny, other, 0)
-        across(zb, sent)
-
-        @pl.when(zb <= zi)
-        def _():
-            upward(zb, sent)
-
-        @pl.when(zb >= zi)
-        def _():
-            downward(zb, sent)
-
-        return 0
-
-    lax.fori_loop(0, nz, settle_row, 0)
-
     def flat(x):
         if c_here % 16:
-            return x.astype(F32).reshape(ns * c_here, HEAD_DIM).astype(BF16)
-        return x.reshape(ns * c_here, HEAD_DIM)
+            return x.astype(F32).reshape(nz * c_here, HEAD_DIM).astype(BF16)
+        return x.reshape(nz * c_here, HEAD_DIM)
 
     far_tile = tokens // 4
 
-    def far(t):
+    def far(t, o, last):
         ids = pl.ds(pl.multiple_of(t * far_tile, 16), far_tile)
+        col = (yi + o) % ny
         for h in range(heads):
             lo = h * HEAD_DIM
-            ck = flat(ctx_all[:, :, lo:lo + HEAD_DIM])
-            cv = flat(ctx_all[:, :, width + lo:width + lo + HEAD_DIM])
+            ck = flat(ctx_all[col, :, :, lo:lo + HEAD_DIM])
+            cv = flat(ctx_all[col, :, :, width + lo:width + lo + HEAD_DIM])
             s = dot_t(q[ids, lo:lo + HEAD_DIM], ck)
             mn = m_near[h, ids, :]
             m = jnp.maximum(jnp.max(s, axis=-1, keepdims=True), mn)
             e = jnp.exp2(s - m)
             w = jnp.exp2(mn - m)
             l = jnp.sum(e, axis=-1, keepdims=True) + w * l_near[h, ids, :]
-            o = dot(e.astype(BF16), cv) + w * o_near[ids, lo:lo + HEAD_DIM]
-            att[ids, lo:lo + HEAD_DIM] = (o / l).astype(BF16)
+            acc = dot(e.astype(BF16), cv) + w * o_near[ids, lo:lo + HEAD_DIM]
+            if last:
+                att[ids, lo:lo + HEAD_DIM] = (acc / l).astype(BF16)
+            else:
+                m_near[h, ids, :] = m
+                l_near[h, ids, :] = l
+                o_near[ids, lo:lo + HEAD_DIM] = acc
+
+    def far_all(o, _):
+        for t in range(4):
+            far(t, o, False)
+        return 0
+
+    if ny > 1:
+        far_all(0, 0)
+
+    def settle_row(zb, _):
+        def other(o, _):
+            arrived(zb * ny + (yi + o) % ny)
+            return 0
+
+        lax.fori_loop(1, ny, other, 0)
+        across(zb, sent)
+
+        @pl.when(zb <= zi)
+        def _():
+            upward(zb, sent)
+
+        @pl.when(zb >= zi)
+        def _():
+            downward(zb, sent)
+
+        return 0
+
+    lax.fori_loop(0, nz, settle_row, 0)
+
+    lax.fori_loop(1, ny - 1, far_all, 0)
 
     def head_copy(src, dst):
         return pltpu.make_async_remote_copy(
@@ -362,16 +384,16 @@
             device_id={"sp": sp, "tp": dst},
         )
 
-    far((1 - my_half) * 2)
-    far((1 - my_half) * 2 + 1)
+    far((1 - my_half) * 2, ny - 1, True)
+    far((1 - my_half) * 2 + 1, ny - 1, True)
 
     def send_other(j, _):
         head_copy(tp, (1 - my_half) * half_t + j).start()
         return 0
 
     lax.fori_loop(0, half_t, send_other, 0)
-    far(my_half * 2)
-    far(my_half * 2 + 1)
+    far(my_half * 2, ny - 1, True)
+    far(my_half * 2 + 1, ny - 1, True)
 
     def mate(o):
         return my_half * half_t + (tp + o) % half_t
@@ -432,7 +454,7 @@
     return pl.pallas_call(
         functools.partial(kernel, ns, nt, ny),
         out_shape=jax.ShapeDtypeStruct((own_n, d), BF16),
-        in_specs=[vmem] * 4 + [hbm] * 9,
+        in_specs=[hbm] * 13,
         out_specs=vmem,
         scratch_shapes=[
             pltpu.VMEM((tokens, d), BF16),
@@ -445,7 +467,7 @@
             pltpu.VMEM((nt, 8, d // 2), F32),
             pltpu.VMEM((nt, 8, d // 8), F32),
             pltpu.VMEM((8, d), F32),
-            pltpu.VMEM((ns, c_here, 2 * width), BF16),
+            pltpu.VMEM((ny, ns // ny, c_here, 2 * width), BF16),
             pltpu.VMEM((tokens + halo, 2 * width), BF16),
             pltpu.VMEM((tokens, width), BF16),
             pltpu.VMEM((heads, 2 * WIN_ROWS - 2, GRID_W, PAIR), F32),
@@ -455,7 +477,11 @@
             pltpu.VMEM((tokens, width), BF16),
             pltpu.VMEM((nt, own_n, width), BF16),
             pltpu.VMEM((2 * WIN_ROWS - 1, heads, PAIR), F32),
-            sem((9,)),
+            pltpu.VMEM((1, d), F32),
+            pltpu.VMEM((1, d), F32),
+            pltpu.VMEM((1, d), F32),
+            pltpu.VMEM(table.shape, F32),
+            sem((13,)),
             sem((nt,)), sem((nt,)), sem((nt,)), sem((nt,)),
             sem((ny + 1, ns // ny)), sem((ns,)),
             sem((2,)), sem((2,)),

time: 40.3 us -> 39.1 us (0.970)
  Pallas kernels: 37.8 us -> 36.9 us
    pallas_call x1, Pallas kernels: 37.8 us -> 36.9 us  [shards(): pl.pallas_call(functools.partial(kernel, ns, nt, ny), out_shape=jax.Shape...]
where the time goes in v3:
time: 39.1 us; the launch traced here: 38.9 us
  Pallas kernels  36.9 us (94%)
  local copies, waits for them, and re-layouts  1.98 us (5%)
    pallas_call x1, Pallas kernels, shards(): pl.pallas_call(functools.partial(kernel, ns, nt, ny), out_shape=jax.Shape...  36.9 us
    unnamed x1, local copies, waits for them, and re-layouts  1.98 us

profile of v3, /device:TPU:9, one launch (start us, length us, event | category | flops | bytes accessed | tf_op | source)
XLA Modules:
  0.0 38.9 jit_solution(1964552550634267493)
XLA Ops:
  0.0 36.9 %shard_map.127 = bf16[160,2048]{1,0:T(8,128)(2,1)} custom-call(f32[1,2048]{1,0:T(1,128)} %bitcast.5, f32[1,2048]{1,0:T(1,128)} %bitcast.6, f32[1,2048]{1,0:T(1,128)} %bitcast.7, f32[15,2,31]{2,1,0:T(2,128)} %bitcast.4, bf16[640,2048]{1,0:T(8,128)(2,1)} %lat_h.1, bf16[96,2048]{1,0:T(8,128)(2,1)} %ctx_h.1, bf16[512,2048]{1,0:T(8,128)(2,1)} %wsh_h.1, ...), custom_call_target="tpu_custom_call" | custom-call | tf_op jit(solution)/shard_map/pallas_call | solution.py:454
  36.9 2.0 %copy.15 = bf16[160,2048]{1,0:T(8,128)(2,1)} copy(bf16[160,2048]{1,0:T(8,128)(2,1)} %shard_map.127) | data formatting | bytes 1310720
